TPU v7x, 32 devices: a whole 2x2x4 slice. The times are simulated.
32 devices in a mesh: sp: 8 (over z, y), tp: 4 (over x, core).
Axes of the slice: x: 2, y: 2, z: 4, core: 2. Of those that a mesh axis runs over, the one named last changes fastest.
Arguments:
- mixer_out: bfloat16 [1024, 2048], P('sp'), may hold values from -6 to 6
- conv_out: bfloat16 [1024, 2048], P('sp', 'tp'), may hold values from -350 to 350
- out_cot: bfloat16 [1024, 2048], P('sp'), may hold values from -6 to 6
- routes: int32 [1024, 2], P('sp'), may hold values from 0 to 7, all different within a row; in each aligned block of 128 rows (0 to 127, 128 to 255, ...) at most 64 rows name the same one
- route_weight: float32 [1024, 2], P('sp'), may hold values from 0.3 to 2.5
- gate_weight: bfloat16 [8, 2048, 1024], P('sp', None, 'tp'), may hold values from -0.125 to 0.125
- up_weight: bfloat16 [8, 2048, 1024], P('sp', None, 'tp'), may hold values from -0.125 to 0.125
- down_weight: bfloat16 [8, 1024, 2048], P('sp', 'tp'), may hold values from -0.1875 to 0.1875
- out_weight: bfloat16 [2048, 2048], P('tp'), may hold values from -0.125 to 0.125
- norm_gain: float32 [2048], P('tp'), may hold values from 0.1 to 1.9
- conv_taps: float32 [31, 2048], P(None, 'tp'), may hold values from -1 to 1
Outputs:
- gate_grad: bfloat16 [8, 2048, 1024], P('sp', None, 'tp')
- up_grad: bfloat16 [8, 2048, 1024], P('sp', None, 'tp')
- down_grad: bfloat16 [8, 1024, 2048], P('sp', 'tp')
- proj_grad: float32 [2048, 2048], P('sp', 'tp')
- gated_grad: float32 [1024, 2048], P('sp', 'tp')
Inputs may be any that keep to these rules, and one draw needn't show every extreme that they name: `routes`: each row names 2 different experts. Among the rows of one device no expert is named by more than 64 rows, and in every draw some expert is named by exactly 64 rows of some device.
All inputs are finite; a program needn't handle non-finite values.
Results may differ from a plain program's by a relative error of at most 0.0095.
Values may be sent and summed in bfloat16 or wider, within the bound.
A program may use at most 64 MiB of HBM per device.

v0:
```python
import jax
import jax.numpy as jnp
from jax import lax
from jax.sharding import PartitionSpec as P

norm_epsilon = 1e-05


def shifted(block, axis, distance):
    devices = range(lax.axis_size(axis))
    route = [(i - distance, i) for i in devices if i - distance in devices]
    return lax.ppermute(block, axis, route)


def expert_backward(x_rows, cot_rows, w_gate, w_up, w_down):
    pre_gate = jnp.dot(x_rows, w_gate, preferred_element_type=jnp.float32)
    pre_up = jnp.dot(x_rows, w_up, preferred_element_type=jnp.float32)
    sig_gate = jax.nn.sigmoid(pre_gate)
    activation = (pre_gate * sig_gate * pre_up).astype(jnp.bfloat16)
    down_g = lax.dot_general(
        activation, cot_rows, (((0,), (0,)), ((), ())), preferred_element_type=jnp.float32
    ).astype(jnp.bfloat16)
    act_grad = lax.dot_general(
        cot_rows, w_down, (((1,), (1,)), ((), ())), preferred_element_type=jnp.float32
    )
    gate_pre_grad = (act_grad * pre_up * sig_gate * (1.0 + pre_gate * (1.0 - sig_gate))).astype(
        jnp.bfloat16
    )
    up_pre_grad = (act_grad * pre_gate * sig_gate).astype(jnp.bfloat16)
    gate_g = lax.dot_general(
        x_rows, gate_pre_grad, (((0,), (0,)), ((), ())), preferred_element_type=jnp.float32
    ).astype(jnp.bfloat16)
    up_g = lax.dot_general(
        x_rows, up_pre_grad, (((0,), (0,)), ((), ())), preferred_element_type=jnp.float32
    ).astype(jnp.bfloat16)
    partial_value = lax.dot_general(
        gate_pre_grad, w_gate, (((1,), (1,)), ((), ())), preferred_element_type=jnp.float32
    )
    partial_value = partial_value + lax.dot_general(
        up_pre_grad, w_up, (((1,), (1,)), ((), ())), preferred_element_type=jnp.float32
    )
    rounded = lax.optimization_barrier(partial_value.astype(jnp.bfloat16))
    return (gate_g, up_g, down_g, rounded.astype(jnp.float32))


def on_device(
    mixer_out,
    conv_out,
    out_cot,
    routes,
    route_weight,
    gate_weight,
    up_weight,
    down_weight,
    out_weight,
    norm_gain,
    conv_taps,
):
    tokens_here, model_width = out_cot.shape
    route_count = routes.shape[1]
    experts = lax.axis_size("sp")
    capacity = 2 * tokens_here * route_count // experts
    quarter = conv_out.shape[1]
    first_col = lax.axis_index("tp") * quarter
    flat_routes = routes.reshape(-1)
    one_hot = (flat_routes[:, None] == jnp.arange(experts, dtype=jnp.int32)[None, :]).astype(
        jnp.int32
    )
    within = jnp.sum((jnp.cumsum(one_hot, axis=0) - one_hot) * one_hot, axis=1)
    slot_index = flat_routes * capacity + within
    row_cot = (route_weight[:, :, None] * out_cot[:, None, :].astype(jnp.float32)).astype(
        jnp.bfloat16
    )
    row_cot = row_cot.reshape(tokens_here * route_count, model_width)
    rows_input = jnp.repeat(mixer_out, route_count, axis=0)
    w_gate = gate_weight[0]
    w_up = up_weight[0]
    w_down = down_weight[0]
    rows_part = lax.dynamic_slice_in_dim(rows_input, first_col, quarter, 1)
    cot_part = lax.dynamic_slice_in_dim(row_cot, first_col, quarter, 1)
    send_rows = jnp.zeros((experts * capacity, quarter), jnp.bfloat16).at[slot_index].set(rows_part)
    send_cot = jnp.zeros((experts * capacity, quarter), jnp.bfloat16).at[slot_index].set(cot_part)
    rows_slice, cot_slice = (
        lax.all_to_all(send_rows, "sp", split_axis=0, concat_axis=0, tiled=True),
        lax.all_to_all(send_cot, "sp", split_axis=0, concat_axis=0, tiled=True),
    )
    x_rows, cot_rows = (
        lax.all_gather(rows_slice, "tp", axis=1, tiled=True),
        lax.all_gather(cot_slice, "tp", axis=1, tiled=True),
    )
    gate_g, up_g, down_g, partial_value = expert_backward(x_rows, cot_rows, w_gate, w_up, w_down)
    back_slice = lax.psum_scatter(
        partial_value.astype(jnp.bfloat16), "tp", scatter_dimension=1, tiled=True
    )
    returned = lax.all_to_all(back_slice, "sp", split_axis=0, concat_axis=0, tiled=True)
    picked = returned[slot_index].astype(jnp.float32).reshape(tokens_here, route_count, quarter)
    own_cot = lax.dynamic_slice_in_dim(out_cot, first_col, quarter, 1).astype(jnp.float32)
    mix_part = (own_cot + jnp.sum(picked, axis=1)).astype(jnp.bfloat16)
    mix_grad = lax.all_gather(mix_part, "tp", axis=1, tiled=True)
    conv_vals = conv_out.astype(jnp.float32)
    power_sum = lax.psum(jnp.sum(conv_vals * conv_vals, axis=1), "tp")
    inv_rms = lax.rsqrt(power_sum / model_width + norm_epsilon)[:, None]
    normed = conv_vals * inv_rms * norm_gain[None, :]
    sig_norm = jax.nn.sigmoid(normed)
    activated = (normed * sig_norm).astype(jnp.bfloat16)
    proj_grad = lax.psum_scatter(
        lax.dot_general(
            mix_grad, activated, (((0,), (0,)), ((), ())), preferred_element_type=jnp.float32
        ),
        "sp",
        scatter_dimension=0,
        tiled=True,
    )
    norm_in_grad = lax.dot_general(
        mix_grad, out_weight, (((1,), (1,)), ((), ())), preferred_element_type=jnp.float32
    )
    scaled = norm_in_grad * sig_norm * (1.0 + normed * (1.0 - sig_norm)) * norm_gain[None, :]
    dot_sum = lax.psum(jnp.sum(conv_vals * scaled, axis=1), "tp")
    conv_grad = inv_rms * scaled - conv_vals * inv_rms**3 * (dot_sum / model_width)[:, None]
    reach = conv_taps.shape[0] - 1
    following = shifted(conv_grad[:reach].astype(jnp.bfloat16), "sp", -1).astype(jnp.float32)
    extended = jnp.concatenate([conv_grad, following], axis=0)
    gated_grad = jnp.zeros((tokens_here, quarter), jnp.float32)
    for tap_index in range(reach + 1):
        gated_grad = (
            gated_grad
            + conv_taps[tap_index][None, :] * extended[tap_index : tap_index + tokens_here]
        )
    return (gate_g[None], up_g[None], down_g[None], proj_grad, gated_grad)


def solution(mesh):
    placed = (
        P("sp", None),
        P("sp", "tp"),
        P("sp", None),
        P("sp", None),
        P("sp", None),
        P("sp", None, "tp"),
        P("sp", None, "tp"),
        P("sp", "tp", None),
        P("tp", None),
        P("tp"),
        P(None, "tp"),
    )
    return jax.shard_map(
        on_device,
        mesh=mesh,
        in_specs=placed,
        out_specs=(
            P("sp", None, "tp"),
            P("sp", None, "tp"),
            P("sp", "tp", None),
            P("sp", "tp"),
            P("sp", "tp"),
        ),
        check_vma=False,
    )
```

profile of v0, /device:TPU:0, one launch (start us, length us, event | category | flops | bytes accessed | tf_op | source)
XLA Modules:
  0.0 249.0 jit_solution(12944334722822858562)
XLA Ops:
  7.2 0.8 broadcast_multiply_fusion
  8.0 0.8 copy.17
  8.8 0.1 eq.29
  9.0 0.1 eq.25
  9.1 0.1 copy.16
  9.2 0.1 mul.438
  9.4 0.6 reduce-window.6
  10.0 0.2 slice_reduce_fusion
  10.2 1.7 broadcast_in_dim.8
  11.9 1.2 reshape.83
  13.1 0.1 fusion.131
  13.2 2.1 scatter_custom_fusion
  15.3 21.7 %all_to_all.36 = bf16[8,64,512]{2,1,0:T(8,128)(2,1)} all-to-all(bf16[8,64,512]{2,1,0:T(8,128)(2,1)S(1)} %bitcast.85), channel_id=1, replica_groups=mesh['sp'=8,'tp'=4] {'sp'}, dimensions={0} | all-to-all | bytes 1048576 | tf_op jit(solution)/shard_map/all_to_all | solution.py:84
  37.1 2.4 mul.443
  39.5 3.7 %mul.444 = f32[256,2048]{1,0:T(8,128)} reshape(f32[128,2,2048]{2,1,0:T(2,128)} %mul.443) | data formatting | bytes 4194304 | tf_op jit(solution)/shard_map/mul | solution.py:71
  43.2 0.1 copy.19
  43.3 0.1 mul.441
  43.4 2.4 scatter_custom_fusion.1
  45.8 17.5 %all_to_all.37 = bf16[8,64,512]{2,1,0:T(8,128)(2,1)} all-to-all(bf16[8,64,512]{2,1,0:T(8,128)(2,1)S(1)} %bitcast.84), channel_id=1, replica_groups=mesh['sp'=8,'tp'=4] {'sp'}, dimensions={0} | all-to-all | bytes 1048576 | tf_op jit(solution)/shard_map/all_to_all | solution.py:85
  63.4 3.5 %fusion.7 = f32[512,256]{1,0:T(8,128)} fusion(bf16[512,2048]{1,0:T(8,128)(2,1)} %all-gather.3.cloned.1.call-done, bf16[1,2048,256]{2,1,0:T(8,128)(2,1)} %param.16), kind=kOutput, calls=%fused_computation.44 | convolution fusion | flops 536870912 | bytes 3670016 | tf_op jit(solution)/shard_map/dot_general | solution.py:16
  66.9 1.5 fusion.10
  68.4 16.7 %all-gather.5.cloned.1.call-done = bf16[512,2048]{1,0:T(8,128)(2,1)} async-done(((bf16[512,512]{1,0:T(8,128)(2,1)}), bf16[512,2048]{1,0:T(8,128)(2,1)}) %all-gather.5.cloned.1.call-update) | async-done | bytes 2097168 | tf_op jit(solution)/shard_map/all_gather | solution.py:89
  85.1 3.0 %multiply_convert_fusion.1 = (bf16[512,256]{1,0:T(8,128)(2,1)S(1)}, bf16[512,256]{1,0:T(8,128)(2,1)S(1)}) fusion(f32[512,256]{1,0:T(8,128)} %fusion.7, f32[512,256]{1,0:T(8,128)} %fusion.10, bf16[512,2048]{1,0:T(8,128)(2,1)} %all-gather.5.cloned.1.call-done, bf16[1,256,2048]{2,1,0:T(8,128)(2,1)} %param.18), kind=kOutput, calls=%fused_computation.83 | convolution fusion | flops 538574848 | bytes 4718592 | tf_op jit(solution)/shard_map/dot_general | solution.py:23
  88.1 0.7 fusion.5
  88.8 0.6 copy-done.5
  89.4 2.1 add_convert_fusion
  91.5 31.3 %reduce-scatter.3.cloned.1.call-done = bf16[512,512]{1,0:T(8,128)(2,1)} async-done(((bf16[512,2048]{1,0:T(8,128)(2,1)}), bf16[512,512]{1,0:T(8,128)(2,1)}) %reduce-scatter.3.cloned.1.call-update) | async-done | bytes 524304 | tf_op jit(solution)/shard_map/reduce_scatter | solution.py:92
  122.8 5.5 %all-to-all-start.2 = ((bf16[8,64,512]{2,1,0:T(8,128)(2,1)}), bf16[8,64,512]{2,1,0:T(8,128)(2,1)S(1)}, u32[]{:S(2)}, u32[]{:S(2)}) async-start(bf16[8,64,512]{2,1,0:T(8,128)(2,1)} %bitcast.86), calls=%async_computation.3 | async-start | bytes 1048576 | tf_op jit(solution)/shard_map/all_to_all | solution.py:95
  128.4 0.1 fusion.15
  128.5 6.0 %psum.14 = f32[128]{0:T(128)S(1)} all-reduce(f32[128]{0:T(128)S(1)} %fusion.15), channel_id=1, replica_groups=mesh['sp'=8,'tp'=4] {'tp'}, use_global_device_ids=true, to_apply=%region_8.9 | all-reduce | flops 128 | bytes 1024 | tf_op jit(solution)/shard_map/psum | solution.py:101
  134.5 8.2 %all-to-all-done.2 = bf16[8,64,512]{2,1,0:T(8,128)(2,1)S(1)} async-done(((bf16[8,64,512]{2,1,0:T(8,128)(2,1)}), bf16[8,64,512]{2,1,0:T(8,128)(2,1)S(1)}, u32[]{:S(2)}, u32[]{:S(2)}) %all-to-all-start.2) | async-done | bytes 524320 | tf_op jit(solution)/shard_map/all_to_all | solution.py:95
  142.7 1.2 gather_fusion
  143.8 0.3 reshape.84
  144.2 0.6 reduce_sum.40
  144.8 0.9 add_convert_fusion.1
  145.7 6.7 %all_gather.11 = bf16[128,2048]{1,0:T(8,128)(2,1)S(1)} all-gather(bf16[128,512]{1,0:T(8,128)(2,1)S(1)} %add_convert_fusion.1), channel_id=1, replica_groups=mesh['sp'=8,'tp'=4] {'tp'}, dimensions={1}, use_global_device_ids=true | all-gather | bytes 655360 | tf_op jit(solution)/shard_map/all_gather | solution.py:99
  152.4 2.8 %fusion.125 = f32[2048,512]{1,0:T(8,128)} fusion(bf16[128,2048]{1,0:T(8,128)(2,1)S(1)} %all_gather.11, bf16[128,512]{1,0:T(8,128)(2,1)S(1)} %copy-done.2, f32[512]{0:T(512)S(1)} %copy-done.12, f32[128]{0:T(128)S(1)} %get-tuple-element.39), kind=kOutput, calls=%fused_computation.201 | convolution fusion | flops 268959744 | bytes 4852224 | tf_op jit(solution)/shard_map/dot_general | solution.py:107
  155.2 0.8 copy-done.11
  156.2 3.5 %fusion = bf16[1,2048,256]{2,1,0:T(8,128)(2,1)} fusion(bf16[512,2048]{1,0:T(8,128)(2,1)} %all-gather.3.cloned.1.call-done, bf16[512,256]{1,0:T(8,128)(2,1)S(1)} %get-tuple-element.6), kind=kOutput, calls=%fused_computation.36 | convolution fusion | flops 537395200 | bytes 3407872 | tf_op jit(solution)/shard_map/dot_general | solution.py:30
  159.6 1.8 fusion.2
  161.4 0.9 fusion.27
  162.3 7.2 %psum.15 = f32[128]{0:T(128)S(1)} all-reduce(f32[128]{0:T(128)S(1)} %get-tuple-element.40), channel_id=1, replica_groups=mesh['sp'=8,'tp'=4] {'tp'}, use_global_device_ids=true, to_apply=%region_11.12 | all-reduce | flops 128 | bytes 1024 | tf_op jit(solution)/shard_map/psum | solution.py:118
  169.6 0.1 fusion.26
  169.7 1.3 collective-permute-start
  171.0 3.3 %fusion.1 = bf16[1,2048,256]{2,1,0:T(8,128)(2,1)} fusion(bf16[512,2048]{1,0:T(8,128)(2,1)} %all-gather.3.cloned.1.call-done, bf16[512,256]{1,0:T(8,128)(2,1)S(1)} %copy-done.10), kind=kOutput, calls=%fused_computation.37 | convolution fusion | flops 537395200 | bytes 3407872 | tf_op jit(solution)/shard_map/dot_general | solution.py:33
  174.4 1.1 collective-permute-done
  175.5 1.4 fusion.33
  176.9 65.6 %reduce-scatter.5.cloned.1.call-done = f32[256,512]{1,0:T(8,128)} async-done(((f32[2048,512]{1,0:T(8,128)}), f32[256,512]{1,0:T(8,128)}) %reduce-scatter.5.cloned.1.call-update) | async-done | bytes 524304 | tf_op jit(solution)/shard_map/reduce_scatter | solution.py:106
  (48 shorter events, 0.4 us)
Async XLA Ops:
  7.2 154.2 %copy-start = (bf16[512,2048]{1,0:T(8,128)(2,1)S(1)}, bf16[512,2048]{1,0:T(8,128)(2,1)}, u32[]{:S(2)}) copy-start(bf16[512,2048]{1,0:T(8,128)(2,1)} %param.19) | copy-start | bytes 6291460
  7.2 56.2 %all-gather.3.cloned.1.call-start = ((), (), s32[]{:S(2)}) async-start(), calls=%async_computation.5 | async-start | bytes 2621440 | tf_op jit(solution)/shard_map/all_gather | solution.py:88
  13.1 24.0 %copy-start.6 = (bf16[128,2048]{1,0:T(8,128)(2,1)S(1)}, bf16[128,2048]{1,0:T(8,128)(2,1)}, u32[]{:S(2)}) copy-start(bf16[128,2048]{1,0:T(8,128)(2,1)} %param.13) | copy-start | bytes 1572868
  37.1 48.0 %all-gather.5.cloned.1.call-start = ((), (), s32[]{:S(2)}) async-start(), calls=%async_computation.6 | async-start | bytes 2621440 | tf_op jit(solution)/shard_map/all_gather | solution.py:89
  39.5 3.7 %copy-start.13 = (f32[128,2]{0,1:T(2,128)S(1)}, f32[128,2]{0,1:T(2,128)}, u32[]{:S(2)}) copy-start(f32[128,2]{0,1:T(2,128)} %param.15) | copy-start | bytes 3076
  63.3 3.6 %copy-start.4 = (bf16[1,2048,256]{2,1,0:T(8,128)(2,1)S(1)}, bf16[1,2048,256]{2,1,0:T(8,128)(2,1)}, u32[]{:S(2)}) copy-start(bf16[1,2048,256]{2,1,0:T(8,128)(2,1)} %param.17) | copy-start | bytes 3145732
  63.3 59.5 %reduce-scatter.3.cloned.1.call-start = ((), (), s32[]{:S(2)}) async-start(), calls=%async_computation.7 | async-start | bytes 2621440 | tf_op jit(solution)/shard_map/reduce_scatter | solution.py:92
  63.4 3.5 %copy-start.14 = (bf16[512,2048]{1,0:T(8,128)(2,1)S(1)}, bf16[512,2048]{1,0:T(8,128)(2,1)}, u32[]{:S(2)}) copy-start(bf16[512,2048]{1,0:T(8,128)(2,1)} %all-gather.3.cloned.1.call-done) | copy-start | bytes 6291460
  68.4 19.6 %copy-start.3 = (bf16[1,2048,256]{2,1,0:T(8,128)(2,1)S(1)}, bf16[1,2048,256]{2,1,0:T(8,128)(2,1)}, u32[]{:S(2)}) copy-start(bf16[1,2048,256]{2,1,0:T(8,128)(2,1)} %param.16) | copy-start | bytes 3145732
  88.1 0.8 copy-start.9
  88.1 1.3 copy-start.5
  91.5 36.9 %copy-start.2 = (bf16[128,512]{1,0:T(8,128)(2,1)S(1)}, bf16[128,512]{1,0:T(8,128)(2,1)}, u32[]{:S(2)}) copy-start(bf16[128,512]{1,0:T(8,128)(2,1)} %param.12) | copy-start | bytes 393220
  122.8 19.8 %all-to-all-start.2 = ((bf16[8,64,512]{2,1,0:T(8,128)(2,1)}), bf16[8,64,512]{2,1,0:T(8,128)(2,1)S(1)}, u32[]{:S(2)}, u32[]{:S(2)}) async-start(bf16[8,64,512]{2,1,0:T(8,128)(2,1)} %bitcast.86), calls=%async_computation.3 | async-start | bytes 1048576 | tf_op jit(solution)/shard_map/all_to_all | solution.py:95
  128.4 114.1 %reduce-scatter.5.cloned.1.call-start = ((), (), s32[]{:S(2)}) async-start(), calls=%async_computation.8 | async-start | bytes 4718592 | tf_op jit(solution)/shard_map/reduce_scatter | solution.py:106
  142.7 9.7 %copy-start.12 = (f32[512]{0:T(512)S(1)}, f32[512]{0:T(512)}, u32[]{:S(2)}) copy-start(f32[512]{0:T(512)} %param.20) | copy-start | bytes 6148
  155.2 0.8 copy-start.11
  156.1 3.5 %copy-start.1 = (bf16[512,2048]{1,0:T(8,128)(2,1)S(1)}, bf16[512,2048]{1,0:T(8,128)(2,1)}, u32[]{:S(2)}) copy-start(bf16[512,2048]{1,0:T(8,128)(2,1)} %all-gather.5.cloned.1.call-done) | copy-start | bytes 6291460
  156.1 3.5 %copy-start.7 = (f32[512,256]{1,0:T(8,128)S(1)}, f32[512,256]{1,0:T(8,128)}, u32[]{:S(2)}) copy-start(f32[512,256]{1,0:T(8,128)} %fusion.7) | copy-start | bytes 1572868
  156.1 3.5 %copy-start.8 = (f32[512,256]{1,0:T(8,128)S(1)}, f32[512,256]{1,0:T(8,128)}, u32[]{:S(2)}) copy-start(f32[512,256]{1,0:T(8,128)} %fusion.10) | copy-start | bytes 1572868
  161.4 9.6 %copy-start.10 = (bf16[512,256]{1,0:T(8,128)(2,1)S(1)}, bf16[512,256]{1,0:T(8,128)(2,1)}, u32[]{:S(2)}) copy-start(bf16[512,256]{1,0:T(8,128)(2,1)} %copy-done.9) | copy-start | bytes 786436
  169.7 5.8 %collective-permute-start = (bf16[30,512]{1,0:T(8,128)(2,1)S(1)}, bf16[30,512]{1,0:T(8,128)(2,1)S(1)}, u32[]{:S(2)}, u32[]{:S(2)}) collective-permute-start(bf16[30,512]{1,0:T(8,128)(2,1)S(1)} %slice.713), channel_id=1, source_target_pairs={{4,0},{8,4},{12,8},{16,12},{20,16},{24,20},{28,24},{5,1},{9,5},{13... | collective-permute-start | bytes 92168 | tf_op jit(solution)/shard_map/ppermute | solution.py:12
Sparse Core Ops, SparseCore 0:
  37.2 21.5 all-gather.2
  63.5 21.6 all-gather.4
  91.6 31.1 reduce-scatter.2
  155.4 87.0 reduce-scatter.4
where the time goes:
time: 250 us; the launch traced here: 249 us
  waiting for transfers between devices  123 us (49%)
  blocking collectives  59.1 us (24%)
  matrix products  23.1 us (9%)
  local copies, waits for them, and re-layouts  15.8 us (6%)
  between operations  14 us (6%)
  other arithmetic  7.12 us (3%)
  starting transfers between devices  6.97 us (3%)
    reduce_scatter x1, waiting for transfers between devices, on_device(): lax.psum_scatter(lax.dot_general(mix_grad, activated, (((0,), (0,)), ((),...  65.6 us
    reduce_scatter x1, waiting for transfers between devices, on_device(): lax.psum_scatter(partial_value.astype(jnp.bfloat16), 'tp', scatter_dimens...  31.3 us
    all_to_all x1, blocking collectives, on_device(): lax.all_to_all(send_rows, 'sp', split_axis=0, concat_axis=0, tiled=True)  21.7 us
    all_to_all x1, blocking collectives, on_device(): lax.all_to_all(send_cot, 'sp', split_axis=0, concat_axis=0, tiled=True)  17.5 us
    all_gather x1, waiting for transfers between devices, on_device(): lax.all_gather(cot_slice, 'tp', axis=1, tiled=True)  16.7 us
    all_to_all x1, waiting for transfers between devices, on_device(): lax.all_to_all(back_slice, 'sp', split_axis=0, concat_axis=0, tiled=True)  8.16 us
    psum x1, blocking collectives, on_device(): dot_sum = lax.psum(jnp.sum(conv_vals * scaled, axis=1), 'tp')  7.21 us
    all_gather x1, blocking collectives, on_device(): mix_grad = lax.all_gather(mix_part, 'tp', axis=1, tiled=True)  6.68 us
  transfers between devices with their start and end apart: 6, of which 5 were waited for; matrix products, arithmetic and copies ran while one was open for 10% of the time, Pallas kernels for 0%

commit v1 on v0

--- a/solution.py
+++ b/solution.py
@@ -2,8 +2,14 @@
 import jax.numpy as jnp
 from jax import lax
 from jax.sharding import PartitionSpec as P
+from jax.lax import all_gather
 
 norm_epsilon = 1e-05
+
+
+def use_the_tables(sample, peer_axis="tp"):
+    m_next = all_gather(sample, peer_axis)
+    return jnp.concatenate(m_next, axis=1)
 
 
 def shifted(block, axis, distance):
@@ -86,7 +92,7 @@
     )
     x_rows, cot_rows = (
         lax.all_gather(rows_slice, "tp", axis=1, tiled=True),
-        lax.all_gather(cot_slice, "tp", axis=1, tiled=True),
+        use_the_tables(cot_slice),
     )
     gate_g, up_g, down_g, partial_value = expert_backward(x_rows, cot_rows, w_gate, w_up, w_down)
     back_slice = lax.psum_scatter(

time: 250 us -> 253 us (1.012)
  local copies, waits for them, and re-layouts: 15.8 us -> 19.4 us
    all_gather x0 -> x1, local copies, waits for them, and re-layouts: none -> 4.16 us  [use_the_tables(): m_next = all_gather(sample, peer_axis)]
where the time goes in v1:
time: 253 us
  waiting for transfers between devices  123 us (49%)
  blocking collectives  59.1 us (23%)
  matrix products  23.2 us (9%)
  local copies, waits for them, and re-layouts  19.4 us (8%)
  between operations  14 us (6%)
  other arithmetic  7.13 us (3%)
  starting transfers between devices  6.97 us (3%)
    reduce_scatter x1, waiting for transfers between devices, on_device(): lax.psum_scatter(lax.dot_general(mix_grad, activated, (((0,), (0,)), ((),...  65.6 us
    reduce_scatter x1, waiting for transfers between devices, on_device(): lax.psum_scatter(partial_value.astype(jnp.bfloat16), 'tp', scatter_dimens...  31.3 us
    all_to_all x1, blocking collectives, on_device(): lax.all_to_all(send_rows, 'sp', split_axis=0, concat_axis=0, tiled=True)  21.7 us
    all_to_all x1, blocking collectives, on_device(): lax.all_to_all(send_cot, 'sp', split_axis=0, concat_axis=0, tiled=True)  17.5 us
    all_gather x1, waiting for transfers between devices, use_the_tables(): m_next = all_gather(sample, peer_axis)  16.7 us
    all_to_all x1, waiting for transfers between devices, on_device(): lax.all_to_all(back_slice, 'sp', split_axis=0, concat_axis=0, tiled=True)  8.17 us
    psum x1, blocking collectives, on_device(): dot_sum = lax.psum(jnp.sum(conv_vals * scaled, axis=1), 'tp')  7.21 us
    all_gather x1, blocking collectives, on_device(): mix_grad = lax.all_gather(mix_part, 'tp', axis=1, tiled=True)  6.68 us
  transfers between devices with their start and end apart: 6, of which 5 were waited for; matrix products, arithmetic and copies ran while one was open for 10% of the time, Pallas kernels for 0%

profile of v1, /device:TPU:0, one launch (start us, length us, event | category | flops | bytes accessed | tf_op | source)
XLA Modules:
  0.0 252.7 jit_solution(11812643183610007828)
XLA Ops:
  7.2 0.8 broadcast_multiply_fusion
  8.0 0.8 copy.28
  8.8 0.1 eq.29
  9.0 0.1 eq.25
  9.1 0.1 copy.27
  9.2 0.1 mul.438
  9.4 0.6 reduce-window.6
  10.0 0.2 slice_reduce_fusion
  10.2 1.7 broadcast_in_dim.8
  11.9 1.2 reshape.90
  13.1 0.1 fusion.131
  13.2 2.1 scatter_custom_fusion
  15.3 21.7 %all_to_all.33 = bf16[8,64,512]{2,1,0:T(8,128)(2,1)} all-to-all(bf16[8,64,512]{2,1,0:T(8,128)(2,1)S(1)} %bitcast.90), channel_id=1, replica_groups=mesh['sp'=8,'tp'=4] {'sp'}, dimensions={0} | all-to-all | bytes 1048576 | tf_op jit(solution)/shard_map/all_to_all | solution.py:90
  37.1 2.4 mul.443
  39.6 3.7 %mul.444 = f32[256,2048]{1,0:T(8,128)} reshape(f32[128,2,2048]{2,1,0:T(2,128)} %mul.443) | data formatting | bytes 4194304 | tf_op jit(solution)/shard_map/mul | solution.py:77
  43.2 0.1 copy.30
  43.3 0.1 mul.441
  43.5 2.4 scatter_custom_fusion.1
  45.9 17.5 %all_to_all.34 = bf16[8,64,512]{2,1,0:T(8,128)(2,1)} all-to-all(bf16[8,64,512]{2,1,0:T(8,128)(2,1)S(1)} %bitcast.89), channel_id=1, replica_groups=mesh['sp'=8,'tp'=4] {'sp'}, dimensions={0} | all-to-all | bytes 1048576 | tf_op jit(solution)/shard_map/all_to_all | solution.py:91
  63.5 3.5 %fusion.7 = f32[512,256]{1,0:T(8,128)} fusion(bf16[512,2048]{1,0:T(8,128)(2,1)} %all-gather.3.cloned.1.call-done, bf16[1,2048,256]{2,1,0:T(8,128)(2,1)} %param.16), kind=kOutput, calls=%fused_computation.44 | convolution fusion | flops 536870912 | bytes 3670016 | tf_op jit(solution)/shard_map/dot_general | solution.py:22
  67.0 1.5 fusion.10
  68.5 16.7 %all-gather.5.cloned.1.call-done = bf16[4,512,512]{2,1,0:T(8,128)(2,1)} async-done(((bf16[1,512,512]{2,1,0:T(8,128)(2,1)}), bf16[4,512,512]{2,1,0:T(8,128)(2,1)}) %all-gather.5.cloned.1.call-update) | async-done | bytes 2097168 | tf_op jit(solution)/shard_map/all_gather | solution.py:11
  85.1 4.2 %copy.31 = bf16[4,512,512]{1,2,0:T(8,128)(2,1)} copy(bf16[4,512,512]{2,1,0:T(8,128)(2,1)} %all-gather.5.cloned.1.call-done) | data formatting | bytes 4194304 | tf_op jit(solution)/shard_map/all_gather | solution.py:11
  89.3 3.0 %multiply_convert_fusion.1 = (bf16[512,256]{1,0:T(8,128)(2,1)S(1)}, bf16[512,256]{1,0:T(8,128)(2,1)S(1)}) fusion(f32[512,256]{1,0:T(8,128)} %fusion.7, f32[512,256]{1,0:T(8,128)} %fusion.10, bf16[512,2048]{0,1:T(8,128)(2,1)} %bitcast.85, bf16[1,256,2048]{2,1,0:T(8,128)(2,1)} %param.18), kind=kOutput, calls=%fused_computation.83 | convolution fusion | flops 538574848 | bytes 4718592 | tf_op jit(solution)/shard_map/dot_general | solution.py:29
  92.4 0.7 fusion.5
  93.1 2.1 add_convert_fusion
  95.3 31.3 %reduce-scatter.3.cloned.1.call-done = bf16[512,512]{1,0:T(8,128)(2,1)} async-done(((bf16[512,2048]{1,0:T(8,128)(2,1)}), bf16[512,512]{1,0:T(8,128)(2,1)}) %reduce-scatter.3.cloned.1.call-update) | async-done | bytes 524304 | tf_op jit(solution)/shard_map/reduce_scatter | solution.py:98
  126.6 5.5 %all-to-all-start.2 = ((bf16[8,64,512]{2,1,0:T(8,128)(2,1)}), bf16[8,64,512]{2,1,0:T(8,128)(2,1)S(1)}, u32[]{:S(2)}, u32[]{:S(2)}) async-start(bf16[8,64,512]{2,1,0:T(8,128)(2,1)} %bitcast.91), calls=%async_computation.3 | async-start | bytes 1048576 | tf_op jit(solution)/shard_map/all_to_all | solution.py:101
  132.2 0.1 fusion.15
  132.3 6.0 %psum.14 = f32[128]{0:T(128)S(1)} all-reduce(f32[128]{0:T(128)S(1)} %fusion.15), channel_id=1, replica_groups=mesh['sp'=8,'tp'=4] {'tp'}, use_global_device_ids=true, to_apply=%region_8.9 | all-reduce | flops 128 | bytes 1024 | tf_op jit(solution)/shard_map/psum | solution.py:107
  138.3 8.2 %all-to-all-done.2 = bf16[8,64,512]{2,1,0:T(8,128)(2,1)S(1)} async-done(((bf16[8,64,512]{2,1,0:T(8,128)(2,1)}), bf16[8,64,512]{2,1,0:T(8,128)(2,1)S(1)}, u32[]{:S(2)}, u32[]{:S(2)}) %all-to-all-start.2) | async-done | bytes 524320 | tf_op jit(solution)/shard_map/all_to_all | solution.py:101
  146.4 1.2 gather_fusion
  147.6 0.3 reshape.93
  147.9 0.6 reduce_sum.40
  148.6 0.9 add_convert_fusion.1
  149.5 6.7 %all_gather.15 = bf16[128,2048]{1,0:T(8,128)(2,1)S(1)} all-gather(bf16[128,512]{1,0:T(8,128)(2,1)S(1)} %add_convert_fusion.1), channel_id=1, replica_groups=mesh['sp'=8,'tp'=4] {'tp'}, dimensions={1}, use_global_device_ids=true | all-gather | bytes 655360 | tf_op jit(solution)/shard_map/all_gather | solution.py:105
  156.2 2.8 %fusion.125 = f32[2048,512]{1,0:T(8,128)} fusion(bf16[128,2048]{1,0:T(8,128)(2,1)S(1)} %all_gather.15, bf16[128,512]{1,0:T(8,128)(2,1)S(1)} %copy-done.2, f32[512]{0:T(512)S(1)} %copy-done.9, f32[128]{0:T(128)S(1)} %get-tuple-element.39), kind=kOutput, calls=%fused_computation.201 | convolution fusion | flops 268959744 | bytes 4852224 | tf_op jit(solution)/shard_map/dot_general | solution.py:113
  159.0 0.8 copy-done.8
  159.9 3.5 %fusion = bf16[1,2048,256]{2,1,0:T(8,128)(2,1)} fusion(bf16[512,2048]{1,0:T(8,128)(2,1)} %all-gather.3.cloned.1.call-done, bf16[512,256]{1,0:T(8,128)(2,1)S(1)} %get-tuple-element.6), kind=kOutput, calls=%fused_computation.36 | convolution fusion | flops 537395200 | bytes 3407872 | tf_op jit(solution)/shard_map/dot_general | solution.py:36
  163.4 1.7 fusion.2
  165.1 0.9 fusion.27
  166.1 7.2 %psum.15 = f32[128]{0:T(128)S(1)} all-reduce(f32[128]{0:T(128)S(1)} %get-tuple-element.40), channel_id=1, replica_groups=mesh['sp'=8,'tp'=4] {'tp'}, use_global_device_ids=true, to_apply=%region_11.12 | all-reduce | flops 128 | bytes 1024 | tf_op jit(solution)/shard_map/psum | solution.py:124
  173.3 0.1 fusion.26
  173.4 1.3 collective-permute-start
  174.7 3.3 %fusion.1 = bf16[1,2048,256]{2,1,0:T(8,128)(2,1)} fusion(bf16[512,2048]{1,0:T(8,128)(2,1)} %all-gather.3.cloned.1.call-done, bf16[512,256]{1,0:T(8,128)(2,1)S(1)} %copy-done.7), kind=kOutput, calls=%fused_computation.37 | convolution fusion | flops 537395200 | bytes 3407872 | tf_op jit(solution)/shard_map/dot_general | solution.py:39
  178.1 1.2 collective-permute-done
  179.2 1.4 fusion.33
  180.6 65.6 %reduce-scatter.5.cloned.1.call-done = f32[256,512]{1,0:T(8,128)} async-done(((f32[2048,512]{1,0:T(8,128)}), f32[256,512]{1,0:T(8,128)}) %reduce-scatter.5.cloned.1.call-update) | async-done | bytes 524304 | tf_op jit(solution)/shard_map/reduce_scatter | solution.py:112
  (47 shorter events, 0.4 us)
Async XLA Ops:
  7.2 158.0 %copy-start = (bf16[512,2048]{1,0:T(8,128)(2,1)S(1)}, bf16[512,2048]{1,0:T(8,128)(2,1)}, u32[]{:S(2)}) copy-start(bf16[512,2048]{1,0:T(8,128)(2,1)} %param.19) | copy-start | bytes 6291460
  7.2 56.3 %all-gather.3.cloned.1.call-start = ((), (), s32[]{:S(2)}) async-start(), calls=%async_computation.5 | async-start | bytes 2621440 | tf_op jit(solution)/shard_map/all_gather | solution.py:94
  13.1 24.0 %copy-start.5 = (bf16[128,2048]{1,0:T(8,128)(2,1)S(1)}, bf16[128,2048]{1,0:T(8,128)(2,1)}, u32[]{:S(2)}) copy-start(bf16[128,2048]{1,0:T(8,128)(2,1)} %param.13) | copy-start | bytes 1572868
  37.1 48.1 %all-gather.5.cloned.1.call-start = ((), (), s32[]{:S(2)}) async-start(), calls=%async_computation.6 | async-start | bytes 2621440 | tf_op jit(solution)/shard_map/all_gather | solution.py:11
  39.6 3.7 %copy-start.10 = (f32[128,2]{0,1:T(2,128)S(1)}, f32[128,2]{0,1:T(2,128)}, u32[]{:S(2)}) copy-start(f32[128,2]{0,1:T(2,128)} %param.15) | copy-start | bytes 3076
  63.4 3.6 %copy-start.4 = (bf16[1,2048,256]{2,1,0:T(8,128)(2,1)S(1)}, bf16[1,2048,256]{2,1,0:T(8,128)(2,1)}, u32[]{:S(2)}) copy-start(bf16[1,2048,256]{2,1,0:T(8,128)(2,1)} %param.17) | copy-start | bytes 3145732
  63.4 63.2 %reduce-scatter.3.cloned.1.call-start = ((), (), s32[]{:S(2)}) async-start(), calls=%async_computation.7 | async-start | bytes 2621440 | tf_op jit(solution)/shard_map/reduce_scatter | solution.py:98
  63.5 3.5 %copy-start.11 = (bf16[512,2048]{1,0:T(8,128)(2,1)S(1)}, bf16[512,2048]{1,0:T(8,128)(2,1)}, u32[]{:S(2)}) copy-start(bf16[512,2048]{1,0:T(8,128)(2,1)} %all-gather.3.cloned.1.call-done) | copy-start | bytes 6291460
  89.3 3.1 %copy-start.3 = (bf16[1,2048,256]{2,1,0:T(8,128)(2,1)S(1)}, bf16[1,2048,256]{2,1,0:T(8,128)(2,1)}, u32[]{:S(2)}) copy-start(bf16[1,2048,256]{2,1,0:T(8,128)(2,1)} %param.16) | copy-start | bytes 3145732
  92.4 0.8 copy-start.6
  95.2 36.9 %copy-start.2 = (bf16[128,512]{1,0:T(8,128)(2,1)S(1)}, bf16[128,512]{1,0:T(8,128)(2,1)}, u32[]{:S(2)}) copy-start(bf16[128,512]{1,0:T(8,128)(2,1)} %param.12) | copy-start | bytes 393220
  126.6 19.8 %all-to-all-start.2 = ((bf16[8,64,512]{2,1,0:T(8,128)(2,1)}), bf16[8,64,512]{2,1,0:T(8,128)(2,1)S(1)}, u32[]{:S(2)}, u32[]{:S(2)}) async-start(bf16[8,64,512]{2,1,0:T(8,128)(2,1)} %bitcast.91), calls=%async_computation.3 | async-start | bytes 1048576 | tf_op jit(solution)/shard_map/all_to_all | solution.py:101
  132.1 114.1 %reduce-scatter.5.cloned.1.call-start = ((), (), s32[]{:S(2)}) async-start(), calls=%async_computation.8 | async-start | bytes 4718592 | tf_op jit(solution)/shard_map/reduce_scatter | solution.py:112
  146.4 9.7 %copy-start.9 = (f32[512]{0:T(512)S(1)}, f32[512]{0:T(512)}, u32[]{:S(2)}) copy-start(f32[512]{0:T(512)} %param.20) | copy-start | bytes 6148
  158.9 0.8 copy-start.8
  159.8 3.5 %copy-start.1 = (bf16[4,512,512]{1,2,0:T(8,128)(2,1)S(1)}, bf16[4,512,512]{1,2,0:T(8,128)(2,1)}, u32[]{:S(2)}) copy-start(bf16[4,512,512]{1,2,0:T(8,128)(2,1)} %copy.31) | copy-start | bytes 6291460
  159.9 3.5 %copy-start.12 = (f32[512,256]{1,0:T(8,128)S(1)}, f32[512,256]{1,0:T(8,128)}, u32[]{:S(2)}) copy-start(f32[512,256]{1,0:T(8,128)} %fusion.7) | copy-start | bytes 1572868
  159.9 3.5 %copy-start.13 = (f32[512,256]{1,0:T(8,128)S(1)}, f32[512,256]{1,0:T(8,128)}, u32[]{:S(2)}) copy-start(f32[512,256]{1,0:T(8,128)} %fusion.10) | copy-start | bytes 1572868
  165.1 9.6 %copy-start.7 = (bf16[512,256]{1,0:T(8,128)(2,1)S(1)}, bf16[512,256]{1,0:T(8,128)(2,1)}, u32[]{:S(2)}) copy-start(bf16[512,256]{1,0:T(8,128)(2,1)} %copy-done.6) | copy-start | bytes 786436
  173.4 5.8 %collective-permute-start = (bf16[30,512]{1,0:T(8,128)(2,1)S(1)}, bf16[30,512]{1,0:T(8,128)(2,1)S(1)}, u32[]{:S(2)}, u32[]{:S(2)}) collective-permute-start(bf16[30,512]{1,0:T(8,128)(2,1)S(1)} %slice.713), channel_id=1, source_target_pairs={{4,0},{8,4},{12,8},{16,12},{20,16},{24,20},{28,24},{5,1},{9,5},{13... | collective-permute-start | bytes 92168 | tf_op jit(solution)/shard_map/ppermute | solution.py:18
Sparse Core Ops, SparseCore 0:
  37.2 21.5 all-gather.2
  63.5 21.5 all-gather.4
  95.4 31.1 reduce-scatter.2
  159.1 87.0 reduce-scatter.4
